TPU v7x, 512 devices: a whole 4x8x8 slice. The times are simulated.
512 devices in a mesh: ep: 32 (over z, x), tp: 16 (over y, core).
Axes of the slice: x: 4, y: 8, z: 8, core: 2. Of those that a mesh axis runs over, the one named last changes fastest.
Arguments:
- first_batch: bfloat16 [65536, 2048], P(('ep', 'tp')), may hold values from -6 to 6
- mixer_gain: float32 [2048], replicated, may hold values from 0.1 to 1.9
- mixer_in: bfloat16 [2048, 512], P(None, 'tp'), may hold values from -0.125 to 0.125
- group_maps: bfloat16 [8, 64, 64], replicated, may hold values from -0.75 to 0.75
- pool_scale: float32 [512], replicated, may hold values from 0.1 to 1.9
- mixer_out: bfloat16 [512, 2048], P('tp'), may hold values from -0.25 to 0.25
- second_batch: bfloat16 [4096, 2048], P('ep'), may hold values from -6 to 6
- expert_gain: float32 [2048], replicated, may hold values from 0.1 to 1.9
- expert_choice: int32 [4096, 2], P('ep'), may hold values from 0 to 31, all different within a row; in each aligned block of 128 rows (0 to 127, 128 to 255, ...) at most 16 rows name the same one
- route_scores: float32 [4096, 2], P('ep'), may hold values from -6 to 6
- expert_gate: bfloat16 [32, 2048, 3584], P('ep', None, 'tp'), may hold values from -0.125 to 0.125
- expert_up: bfloat16 [32, 2048, 3584], P('ep', None, 'tp'), may hold values from -0.125 to 0.125
- expert_down: bfloat16 [32, 3584, 2048], P('ep', 'tp'), may hold values from -0.09375 to 0.09375
Outputs:
- mixed_first: bfloat16 [65536, 2048], P(('ep', 'tp'))
- experts_second: bfloat16 [4096, 2048], P('ep')
Inputs may be any that keep to these rules, and one draw needn't show every extreme that they name: `expert_choice`: the two entries of a row differ. Within the rows of one device (aligned blocks of 128 rows) no expert is named more than 16 times, a bound that some block reaches there.
All inputs are finite; a program needn't handle non-finite values.
Results may differ from a plain program's by a relative error of at most 0.018.
Values may be sent and summed in bfloat16 or wider, within the bound.
No kernel may reach another device: no remote copies, remote signals or barrier semaphores. Data moves between devices by JAX's collectives and lax.ppermute only.
A program may use at most 64 MiB of HBM per device.

v0:
```python
import jax
import jax.numpy as jnp
from jax import lax
from jax.sharding import Mesh
from jax.sharding import PartitionSpec as P

GROUP = 64
SEQS = 1
EP_TP = ("ep_0", "ep_1", "tp")
EP = ("ep_0", "ep_1")
epsilon = 1e-06


def extended(block, sides, width):
    for axis, dim in sides:
        count = lax.axis_size(axis)
        forward = [(i, i + 1) for i in range(count - 1)]
        backward = [(target, source) for source, target in forward]
        low = lax.ppermute(
            lax.slice_in_dim(block, block.shape[dim] - width, None, axis=dim), axis, forward
        )
        high = lax.ppermute(lax.slice_in_dim(block, 0, width, axis=dim), axis, backward)
        block = jnp.concatenate([low, block, high], axis=dim)
    return block


def split_up(shard, dim, peers):
    lengths = shard.shape
    blocks = shard.reshape(*lengths[:dim], peers, lengths[dim] // peers, *lengths[dim + 1 :])
    return jnp.moveaxis(blocks, dim, 0)


def summed_on_arrival(shard, axis, dim):
    peers = lax.axis_size(axis)
    blocks = lax.all_to_all(split_up(shard, dim, peers), axis, 0, 0, tiled=True)
    return jnp.sum(blocks.astype(jnp.float32), axis=0)


def laid_out(blocks, dim):
    lengths = list(blocks.shape[1:])
    lengths[dim] *= blocks.shape[0]
    return jnp.moveaxis(blocks, 0, dim).reshape(lengths)


def moved_by_axis(blocks, axes, turns):
    inside = blocks.shape[1:]
    out = blocks.reshape(*(lax.axis_size(a) for a in axes), *inside)
    for k in turns:
        out = lax.all_to_all(out, axes[k], k, k, tiled=True)
    return out.reshape(-1, *inside)


def stepwise_exchange(shard, axes, turns, split_dim, concat_dim):
    blocks = split_up(shard, split_dim, lax.axis_size(axes))
    return laid_out(moved_by_axis(blocks, axes, turns), concat_dim)


def rms_scale(values, gain):
    floats = values.astype(jnp.float32)
    factor = lax.rsqrt(jnp.mean(floats * floats, axis=-1, keepdims=True) + epsilon)
    return (floats * factor * gain).astype(jnp.bfloat16)


def mixer_half(first_batch, mixer_gain, mixer_in, group_maps, pool_scale, mixer_out):
    count_rows = first_batch.shape[0]
    normed = rms_scale(first_batch, mixer_gain)
    pooled_in = jnp.dot(
        normed,
        lax.all_gather(mixer_in, "tp", axis=1, tiled=True),
        preferred_element_type=jnp.float32,
    ).astype(jnp.bfloat16)
    channels = pooled_in.shape[1]
    padded = extended(pooled_in, ((EP_TP, 0),), 8).astype(jnp.float32)
    devices = lax.axis_size(EP) * lax.axis_size("tp")
    seq_length = count_rows * devices // SEQS
    first_row = (lax.axis_index(EP) * lax.axis_size("tp") + lax.axis_index("tp")) * count_rows
    places = first_row + jnp.arange(count_rows, dtype=jnp.int32)
    own_seq = places // seq_length
    group_of = jnp.arange(channels, dtype=jnp.int32) // GROUP
    half_span = jnp.left_shift(jnp.ones_like(group_of), group_of % 4)
    window_sum = jnp.zeros((count_rows, channels), jnp.float32)
    window_count = jnp.zeros((count_rows, channels), jnp.float32)
    for offset in range(-8, 8):
        inside = (
            ((places + offset) // seq_length == own_seq)[:, None]
            & (offset >= -half_span)[None, :]
            & (offset < half_span)[None, :]
        )
        window_sum = window_sum + jnp.where(
            inside, padded[8 + offset : 8 + offset + count_rows], 0.0
        )
        window_count = window_count + inside.astype(jnp.float32)
    centred = (window_sum / window_count - padded[8 : 8 + count_rows]).astype(jnp.bfloat16)
    group_count = group_maps.shape[0]
    identity = jnp.eye(group_count, dtype=jnp.bfloat16)
    block_map = jnp.einsum("gcd,gh->gchd", group_maps, identity).reshape(channels, channels)
    grouped = (jnp.dot(centred, block_map, preferred_element_type=jnp.float32) * pool_scale).astype(
        jnp.bfloat16
    )
    mixed_out = jnp.dot(
        grouped,
        lax.all_gather(mixer_out, "tp", axis=0, tiled=True),
        preferred_element_type=jnp.float32,
    )
    return mixed_out.astype(jnp.bfloat16)


def expert_half(
    second_batch, expert_gain, expert_choice, route_scores, expert_gate, expert_up, expert_down
):
    row_count = second_batch.shape[0]
    model_width = second_batch.shape[1]
    experts = lax.axis_size(EP)
    tp_count = lax.axis_size("tp")
    capacity = 4 * row_count // experts
    share = capacity // tp_count
    normed = rms_scale(second_batch, expert_gain)
    chosen = expert_choice.reshape(-1)
    one_hot = (chosen[:, None] == jnp.arange(experts, dtype=jnp.int32)[None, :]).astype(jnp.int32)
    ranking = jnp.sum(jnp.cumsum(one_hot, axis=0) * one_hot, axis=1) - 1
    slot_place = ranking * experts + chosen
    source_row = jnp.arange(chosen.shape[0], dtype=jnp.int32) // expert_choice.shape[1]
    slot_table = jnp.zeros((capacity * experts,), jnp.int32).at[slot_place].set(source_row + 1)
    outgoing = jnp.where(
        (slot_table > 0)[:, None],
        normed[jnp.maximum(slot_table - 1, 0)],
        jnp.zeros((), jnp.bfloat16),
    )
    outgoing = outgoing.reshape(capacity, experts, model_width)
    arrived = lax.all_to_all(outgoing, EP, split_axis=1, concat_axis=1, tiled=True)
    incoming = arrived.reshape(capacity * experts, model_width)
    gate_weight = expert_gate[0]
    up_weight = expert_up[0]
    down_weight = expert_down[0]
    gate_part = jnp.dot(incoming, gate_weight, preferred_element_type=jnp.float32)
    up_part = jnp.dot(incoming, up_weight, preferred_element_type=jnp.float32)
    hidden = (jax.nn.silu(gate_part) * up_part).astype(jnp.bfloat16)
    summed = summed_on_arrival(
        jnp.dot(hidden, down_weight, preferred_element_type=jnp.float32).astype(jnp.bfloat16),
        "tp",
        0,
    )
    finished = summed.astype(jnp.bfloat16).reshape(share, experts, model_width)
    returned = stepwise_exchange(finished, EP, (0, 1), 1, 1)
    every_slot = lax.all_gather(returned, "tp", axis=0, tiled=True).reshape(
        capacity * experts, model_width
    )
    picked = every_slot[slot_place].reshape(row_count, -1, model_width)
    weight_first = jax.nn.sigmoid(route_scores[:, 0] - route_scores[:, 1])[:, None]
    blended = weight_first * picked[:, 0].astype(jnp.float32) + (1.0 - weight_first) * picked[
        :, 1
    ].astype(jnp.float32)
    return blended.astype(jnp.bfloat16)


def per_device(
    first_batch,
    mixer_gain,
    mixer_in,
    group_maps,
    pool_scale,
    mixer_out,
    second_batch,
    expert_gain,
    expert_choice,
    route_scores,
    expert_gate,
    expert_up,
    expert_down,
):
    mixed_first = mixer_half(first_batch, mixer_gain, mixer_in, group_maps, pool_scale, mixer_out)
    experts_second = expert_half(
        second_batch, expert_gain, expert_choice, route_scores, expert_gate, expert_up, expert_down
    )
    return (mixed_first, experts_second)


def solution(mesh):
    torus = Mesh(mesh.devices.reshape(8, 4, mesh.shape["tp"]), ("ep_0", "ep_1", "tp"))
    placed = (
        P(EP_TP, None),
        P(),
        P(None, "tp"),
        P(),
        P(),
        P("tp", None),
        P(EP, None),
        P(),
        P(EP, None),
        P(EP, None),
        P(EP, None, "tp"),
        P(EP, None, "tp"),
        P(EP, "tp", None),
    )
    return jax.shard_map(
        per_device,
        mesh=torus,
        in_specs=placed,
        out_specs=(P(EP_TP, None), P(EP, None)),
        check_vma=False,
    )
```

profile of v0, /device:TPU:1, one launch (start us, length us, event | category | flops | bytes accessed | tf_op | source)
XLA Modules:
  0.0 232.5 jit_solution(14111558558822395541)
XLA Ops:
  7.2 0.9 copy.31
  8.0 0.1 eq.156
  8.2 0.1 eq.152
  8.3 0.1 reshape.528
  8.5 0.6 reduce-window.6
  9.1 0.2 slice_reduce_fusion
  9.3 0.1 fusion.142
  9.4 1.4 scatter_custom_fusion
  10.9 1.2 fusion.5
  12.1 0.1 broadcast_in_dim.32
  12.2 0.1 copy.35
  12.3 1.2 fusion.7
  13.5 2.5 %gather_fusion = bf16[512,2048]{1,0:T(8,128)(2,1)S(1)} fusion(bf16[128,2048]{1,0:T(8,128)(2,1)S(1)} %fusion.7, s32[1024]{0:T(1024)S(1)} %pad_clamp_fusion.1), kind=kCustom, calls=%fused_computation | custom fusion | bytes 4196352 | tf_op jit(solution)/shard_map/gather | solution.py:126
  16.0 3.8 %copy_select_fusion = bf16[16,32,2048]{2,0,1:T(8,128)(2,1)} fusion(bf16[16,32,2048]{2,1,0:T(8,128)(2,1)S(1)} %bitcast.56, pred[16,32]{0,1:T(8,128)(4,1)S(1)} %copy.35), kind=kLoop, calls=%fused_computation.5 | loop fusion | flops 1048576 | bytes 4194816 | tf_op jit(solution)/shard_map/jit(_where)/select_n | solution.py:124
  19.8 13.7 %all-to-all-start = ((bf16[16,32,2048]{2,0,1:T(8,128)(2,1)}), bf16[16,32,2048]{2,0,1:T(8,128)(2,1)S(1)}, u32[]{:S(2)}, u32[]{:S(2)}) async-start(bf16[16,32,2048]{2,0,1:T(8,128)(2,1)} %copy_select_fusion), calls=%async_computation | async-start | bytes 4194304 | tf_op jit(solution)/shard_map/all_to_all | solution.py:130
  33.6 0.7 all-gather.4.cloned.1.call-update
  34.2 47.7 %all-to-all-done = bf16[16,32,2048]{2,0,1:T(8,128)(2,1)S(1)} async-done(((bf16[16,32,2048]{2,0,1:T(8,128)(2,1)}), bf16[16,32,2048]{2,0,1:T(8,128)(2,1)S(1)}, u32[]{:S(2)}, u32[]{:S(2)}) %all-to-all-start) | async-done | bytes 2097184 | tf_op jit(solution)/shard_map/all_to_all | solution.py:130
  82.0 1.2 copy.37
  83.1 1.3 copy-done.1
  84.5 0.8 fusion.13
  85.3 0.3 copy-done.6
  85.6 4.5 %convolution_convert_fusion = bf16[512,2048]{1,0:T(8,128)(2,1)} fusion(bf16[512,2048]{1,0:T(8,128)(2,1)} %bitcast.59, bf16[1,224,2048]{2,1,0:T(8,128)(2,1)S(1)} %copy-done, bf16[1,2048,224]{1,2,0:T(8,128)(2,1)S(1)} %copy-done.6, f32[512,224]{0,1:T(8,128)S(1)} %fusion.13), kind=kOutput, calls=%fused_computation.3 | convolution fusion | flops 941260800 | bytes 6488064 | tf_op jit(solution)/shard_map/dot_general | solution.py:139
  90.1 9.8 %all-to-all-start.1 = ((bf16[16,32,2048]{2,1,0:T(8,128)(2,1)}), bf16[16,32,2048]{2,1,0:T(8,128)(2,1)S(1)}, u32[]{:S(2)}, u32[]{:S(2)}) async-start(bf16[16,32,2048]{2,1,0:T(8,128)(2,1)} %bitcast.57), calls=%async_computation.1 | async-start | bytes 4194304 | tf_op jit(solution)/shard_map/all_to_all | solution.py:35
  99.9 0.7 all-gather.6.cloned.1.call-update
  100.8 56.7 %all-to-all-done.1 = bf16[16,32,2048]{2,1,0:T(8,128)(2,1)S(1)} async-done(((bf16[16,32,2048]{2,1,0:T(8,128)(2,1)}), bf16[16,32,2048]{2,1,0:T(8,128)(2,1)S(1)}, u32[]{:S(2)}, u32[]{:S(2)}) %all-to-all-start.1) | async-done | bytes 2097184 | tf_op jit(solution)/shard_map/all_to_all | solution.py:35
  157.5 0.4 reduce_sum.42
  157.9 0.7 reshape_transpose_reshape_reshape.3
  158.6 3.7 %all-to-all-start.2 = ((bf16[8,4,1,1,2048]{4,1,3,2,0:T(4,128)(2,1)}), bf16[8,4,1,1,2048]{4,1,3,2,0:T(4,128)(2,1)S(1)}, u32[]{:S(2)}, u32[]{:S(2)}) async-start(bf16[8,4,1,1,2048]{4,1,3,2,0:T(4,128)(2,1)} %reshape_transpose_reshape_reshape.3), calls=%async_computation.2 | async-start | bytes 262144 | tf_op jit(solution)/shard_map/all_to_all | solution.py:49
  162.4 7.9 %all-to-all-done.2 = bf16[8,4,1,1,2048]{4,1,3,2,0:T(4,128)(2,1)S(1)} async-done(((bf16[8,4,1,1,2048]{4,1,3,2,0:T(4,128)(2,1)}), bf16[8,4,1,1,2048]{4,1,3,2,0:T(4,128)(2,1)S(1)}, u32[]{:S(2)}, u32[]{:S(2)}) %all-to-all-start.2) | async-done | bytes 131104 | tf_op jit(solution)/shard_map/all_to_all | solution.py:49
  170.3 0.7 copy.38
  171.0 3.5 %all-to-all-start.3 = ((bf16[8,4,1,1,2048]{4,0,3,2,1:T(8,128)(2,1)}), bf16[8,4,1,1,2048]{4,0,3,2,1:T(8,128)(2,1)S(1)}, u32[]{:S(2)}, u32[]{:S(2)}) async-start(bf16[8,4,1,1,2048]{4,0,3,2,1:T(8,128)(2,1)} %copy.38), calls=%async_computation.3 | async-start | bytes 262144 | tf_op jit(solution)/shard_map/all_to_all | solution.py:49
  174.5 0.1 all-gather.8.cloned.1.call-start
  174.6 4.7 %all-to-all-done.3 = bf16[8,4,1,1,2048]{4,0,3,2,1:T(8,128)(2,1)S(1)} async-done(((bf16[8,4,1,1,2048]{4,0,3,2,1:T(8,128)(2,1)}), bf16[8,4,1,1,2048]{4,0,3,2,1:T(8,128)(2,1)S(1)}, u32[]{:S(2)}, u32[]{:S(2)}) %all-to-all-start.3) | async-done | bytes 131104 | tf_op jit(solution)/shard_map/all_to_all | solution.py:49
  179.3 0.1 copy.39
  179.4 0.7 reshape_transpose_reshape.3
  180.4 0.2 fusion.2
  180.6 0.2 multiply_bitcast_fusion
  180.8 2.4 %convolution_convert_fusion.2 = bf16[128,512]{1,0:T(8,128)(2,1)S(1)} fusion(bf16[2048,512]{0,1:T(8,128)(2,1)} %all-gather.4.cloned.1.call-done, bf16[128,2048]{1,0:T(8,128)(2,1)S(1)} %copy-done.2, f32[2048]{0:T(1024)S(1)} %copy-done.7, f32[128]{0:T(128)S(1)} %add_rsqrt_fusion.1), kind=kOutput, calls=%fused_computation.14 | convolution fusion | flops 269549568 | bytes 2761216 | tf_op jit(solution)/shard_map/dot_general | solution.py:67
  183.3 6.1 %collective-permute-start = (bf16[8,512]{1,0:T(8,128)(2,1)S(1)}, bf16[8,512]{1,0:T(8,128)(2,1)S(1)}, u32[]{:S(2)}, u32[]{:S(2)}) collective-permute-start(bf16[8,512]{1,0:T(8,128)(2,1)S(1)} %get-tuple-element.6), channel_id=1, source_target_pairs={{0,1},{1,2},{2,3},{3,4},{4,5},{5,6},{6,7},{7,8},{8,9},{9,10},{10,1... | collective-permute-start | bytes 24584 | tf_op jit(solution)/shard_map/ppermute | solution.py:19
  189.4 1.9 collective-permute-start.1
  191.3 0.6 reshape.526
  192.0 2.5 %collective-permute-done.1 = bf16[8,512]{1,0:T(8,128)(2,1)S(1)} collective-permute-done((bf16[8,512]{1,0:T(8,128)(2,1)S(1)}, bf16[8,512]{1,0:T(8,128)(2,1)S(1)}, u32[]{:S(2)}, u32[]{:S(2)}) %collective-permute-start.1) | collective-permute-done | bytes 8224 | tf_op jit(solution)/shard_map/ppermute | solution.py:22
  194.5 4.2 %convolution_convert_fusion.1 = bf16[128,2048]{1,0:T(8,128)(2,1)} fusion(bf16[512,2048]{1,0:T(8,128)(2,1)} %all-gather.6.cloned.1.call-done, bf16[512,512]{1,0:T(8,128)(2,1)S(1)} %reshape.526, f32[144,512]{1,0:T(8,128)S(1)} %maximum_convert_fusion, f32[512]{0:T(512)S(1)} %copy-done.8, f32[512]{0:T(512)S(1)} %get-tuple-element.53, ...), kind=kOutput, calls=%fused_computation.4 | convolution fusion | flops 342097920 | bytes 7367680 | tf_op jit(solution)/shard_map/dot_general | solution.py:100
  198.8 18.9 %all-gather.8.cloned.1.call-done = bf16[16,32,2048]{2,1,0:T(8,128)(2,1)} async-done(((bf16[1,32,2048]{2,1,0:T(8,128)(2,1)}), bf16[16,32,2048]{2,1,0:T(8,128)(2,1)}) %all-gather.8.cloned.1.call-update) | async-done | bytes 2097168 | tf_op jit(solution)/shard_map/all_gather | solution.py:145
  217.7 4.2 %gather_fusion.1 = bf16[256,2048]{1,0:T(8,128)(2,1)S(1)} fusion(bf16[512,2048]{1,0:T(8,128)(2,1)} %bitcast.55, s32[1024]{0:T(1024)S(1)} %pad_clamp_fusion), kind=kCustom, calls=%fused_computation.1 | custom fusion | bytes 2098176 | tf_op jit(solution)/shard_map/gather | solution.py:148
  221.9 0.7 reshape.532
  222.7 1.5 fusion.173
  224.2 1.8 fusion.9
  (62 shorter events, 0.6 us)
Async XLA Ops:
  7.2 78.1 %copy-start = (bf16[1,224,2048]{2,1,0:T(8,128)(2,1)S(1)}, bf16[1,224,2048]{2,1,0:T(8,128)(2,1)}, u32[]{:S(2)}) copy-start(bf16[1,224,2048]{2,1,0:T(8,128)(2,1)} %param.25) | copy-start | bytes 2752516
  19.8 62.2 %all-to-all-start = ((bf16[16,32,2048]{2,0,1:T(8,128)(2,1)}), bf16[16,32,2048]{2,0,1:T(8,128)(2,1)S(1)}, u32[]{:S(2)}, u32[]{:S(2)}) async-start(bf16[16,32,2048]{2,0,1:T(8,128)(2,1)} %copy_select_fusion), calls=%async_computation | async-start | bytes 4194304 | tf_op jit(solution)/shard_map/all_to_all | solution.py:130
  33.5 147.3 %all-gather.4.cloned.1.call-start = ((), (), s32[]{:S(2)}) async-start(), calls=%async_computation.4 | async-start | bytes 2228224 | tf_op jit(solution)/shard_map/all_gather | solution.py:69
  82.0 2.5 %copy-start.5 = (bf16[1,2048,224]{1,2,0:T(8,128)(2,1)S(1)}, bf16[1,2048,224]{1,2,0:T(8,128)(2,1)}, u32[]{:S(2)}) copy-start(bf16[1,2048,224]{1,2,0:T(8,128)(2,1)} %param.23) | copy-start | bytes 2752516
  83.1 1.3 copy-start.1
  84.5 1.2 copy-start.6
  90.1 67.3 %all-to-all-start.1 = ((bf16[16,32,2048]{2,1,0:T(8,128)(2,1)}), bf16[16,32,2048]{2,1,0:T(8,128)(2,1)S(1)}, u32[]{:S(2)}, u32[]{:S(2)}) async-start(bf16[16,32,2048]{2,1,0:T(8,128)(2,1)} %bitcast.57), calls=%async_computation.1 | async-start | bytes 4194304 | tf_op jit(solution)/shard_map/all_to_all | solution.py:35
  99.9 94.6 %all-gather.6.cloned.1.call-start = ((), (), s32[]{:S(2)}) async-start(), calls=%async_computation.5 | async-start | bytes 2228224 | tf_op jit(solution)/shard_map/all_gather | solution.py:102
  100.7 79.8 %copy-start.4 = (f32[128,2]{0,1:T(2,128)S(1)}, f32[128,2]{0,1:T(2,128)}, u32[]{:S(2)}) copy-start(f32[128,2]{0,1:T(2,128)} %param.22) | copy-start | bytes 3076
  100.8 79.8 %copy-start.3 = (bf16[8,64,64]{2,1,0:T(8,128)(2,1)S(1)}, bf16[8,64,64]{2,1,0:T(8,128)(2,1)}, u32[]{:S(2)}) copy-start(bf16[8,64,64]{2,1,0:T(8,128)(2,1)} %param.16) | copy-start | bytes 196612
  157.9 22.5 %copy-start.2 = (bf16[128,2048]{1,0:T(8,128)(2,1)S(1)}, bf16[128,2048]{1,0:T(8,128)(2,1)}, u32[]{:S(2)}) copy-start(bf16[128,2048]{1,0:T(8,128)(2,1)} %param.13) | copy-start | bytes 1572868
  157.9 22.9 %copy-start.7 = (f32[2048]{0:T(1024)S(1)}, f32[2048]{0:T(1024)}, u32[]{:S(2)}) copy-start(f32[2048]{0:T(1024)} %param.14) | copy-start | bytes 24580
  158.6 11.6 %all-to-all-start.2 = ((bf16[8,4,1,1,2048]{4,1,3,2,0:T(4,128)(2,1)}), bf16[8,4,1,1,2048]{4,1,3,2,0:T(4,128)(2,1)S(1)}, u32[]{:S(2)}, u32[]{:S(2)}) async-start(bf16[8,4,1,1,2048]{4,1,3,2,0:T(4,128)(2,1)} %reshape_transpose_reshape_reshape.3), calls=%async_computation.2 | async-start | bytes 262144 | tf_op jit(solution)/shard_map/all_to_all | solution.py:49
  171.0 8.3 %all-to-all-start.3 = ((bf16[8,4,1,1,2048]{4,0,3,2,1:T(8,128)(2,1)}), bf16[8,4,1,1,2048]{4,0,3,2,1:T(8,128)(2,1)S(1)}, u32[]{:S(2)}, u32[]{:S(2)}) async-start(bf16[8,4,1,1,2048]{4,0,3,2,1:T(8,128)(2,1)} %copy.38), calls=%async_computation.3 | async-start | bytes 262144 | tf_op jit(solution)/shard_map/all_to_all | solution.py:49
  174.5 43.2 %all-gather.8.cloned.1.call-start = ((), (), s32[]{:S(2)}) async-start(), calls=%async_computation.6 | async-start | bytes 2228224 | tf_op jit(solution)/shard_map/all_gather | solution.py:145
  180.8 13.8 %copy-start.8 = (f32[512]{0:T(512)S(1)}, f32[512]{0:T(512)}, u32[]{:S(2)}) copy-start(f32[512]{0:T(512)} %param.17) | copy-start | bytes 6148
  183.3 8.7 %collective-permute-start = (bf16[8,512]{1,0:T(8,128)(2,1)S(1)}, bf16[8,512]{1,0:T(8,128)(2,1)S(1)}, u32[]{:S(2)}, u32[]{:S(2)}) collective-permute-start(bf16[8,512]{1,0:T(8,128)(2,1)S(1)} %get-tuple-element.6), channel_id=1, source_target_pairs={{0,1},{1,2},{2,3},{3,4},{4,5},{5,6},{6,7},{7,8},{8,9},{9,10},{10,1... | collective-permute-start | bytes 24584 | tf_op jit(solution)/shard_map/ppermute | solution.py:19
  189.4 5.1 %collective-permute-start.1 = (bf16[8,512]{1,0:T(8,128)(2,1)S(1)}, bf16[8,512]{1,0:T(8,128)(2,1)S(1)}, u32[]{:S(2)}, u32[]{:S(2)}) collective-permute-start(bf16[8,512]{1,0:T(8,128)(2,1)S(1)} %get-tuple-element.7), channel_id=1, source_target_pairs={{1,0},{2,1},{3,2},{4,3},{5,4},{6,5},{7,6},{8,7},{9,8},{10,9},{11,1... | collective-permute-start | bytes 24584 | tf_op jit(solution)/shard_map/ppermute | solution.py:22
Sparse Core Ops, SparseCore 0:
  36.4 43.6 all-gather.3
  102.8 57.5 all-gather.5
  180.2 37.4 all-gather.7
where the time goes:
time: 233 us; the launch traced here: 232 us
  waiting for transfers between devices  140 us (60%)
  starting transfers between devices  38.8 us (17%)
  local copies, waits for them, and re-layouts  17.7 us (8%)
  between operations  14.2 us (6%)
  matrix products  12 us (5%)
  other arithmetic  9.87 us (4%)
    all_to_all x1, waiting for transfers between devices, summed_on_arrival(): blocks = lax.all_to_all(split_up(shard, dim, peers), axis, 0, 0, tiled=True)  56.7 us
    all_to_all x1, waiting for transfers between devices, expert_half(): lax.all_to_all(outgoing, EP, split_axis=1, concat_axis=1, tiled=True)  47.7 us
    all_gather x1, waiting for transfers between devices, expert_half(): lax.all_gather(returned, 'tp', axis=0, tiled=True)  18.9 us
    all_to_all x1, starting transfers between devices, expert_half(): lax.all_to_all(outgoing, EP, split_axis=1, concat_axis=1, tiled=True)  13.7 us
    all_to_all x2, waiting for transfers between devices, moved_by_axis(): out = lax.all_to_all(out, axes[k], k, k, tiled=True)  12.6 us
    all_to_all x1, starting transfers between devices, summed_on_arrival(): blocks = lax.all_to_all(split_up(shard, dim, peers), axis, 0, 0, tiled=True)  9.75 us
    all_to_all x2, starting transfers between devices, moved_by_axis(): out = lax.all_to_all(out, axes[k], k, k, tiled=True)  7.19 us
    ppermute x1, starting transfers between devices, extended(): lax.ppermute(lax.slice_in_dim(block, block.shape[dim] - width, None, axis...  6.09 us
  transfers between devices with their start and end apart: 9, of which 6 were waited for; matrix products, arithmetic and copies ran while one was open for 7% of the time, Pallas kernels for 0%

commit v1 on v0

--- a/solution.py
+++ b/solution.py
@@ -142,9 +142,9 @@
     )
     finished = summed.astype(jnp.bfloat16).reshape(share, experts, model_width)
     returned = stepwise_exchange(finished, EP, (0, 1), 1, 1)
-    every_slot = lax.all_gather(returned, "tp", axis=0, tiled=True).reshape(
-        capacity * experts, model_width
-    )
+    every_slot = jnp.concatenate(
+        lax.all_to_all(jnp.stack([returned] * lax.axis_size("tp")), "tp", 0, 0), axis=0
+    ).reshape(capacity * experts, model_width)
     picked = every_slot[slot_place].reshape(row_count, -1, model_width)
     weight_first = jax.nn.sigmoid(route_scores[:, 0] - route_scores[:, 1])[:, None]
     blended = weight_first * picked[:, 0].astype(jnp.float32) + (1.0 - weight_first) * picked[

time: 233 us -> 261 us (1.12)
  other arithmetic: 9.87 us -> 28.1 us
  starting transfers between devices: 38.8 us -> 44.8 us
    ppermute x1, waiting for transfers between devices: 0.01 us -> 22.3 us  [extended(): lax.ppermute(lax.slice_in_dim(block, block.shape[dim] - width, None, axis...]
    all_gather x1 -> x0, waiting for transfers between devices: 18.9 us -> none  [expert_half(): lax.all_gather(returned, 'tp', axis=0, tiled=True)]
    all_to_all x0 -> x1, starting transfers between devices: none -> 8.65 us  [expert_half(): lax.all_to_all(jnp.stack([returned] * lax.axis_size('tp')), 'tp', 0, 0)]
    le x14, other arithmetic: 0.12 us -> 7.9 us  [mixer_half(): offset >= -half_span]
    eq x8, other arithmetic: 0.13 us -> 4.74 us  [mixer_half(): (places + offset) // seq_length == own_seq]
  transfers between devices with their start and end apart: 9 -> 9, of which waited for: 6 -> 6; matrix products, arithmetic and copies ran while one was open for 7% -> 16% of each run, Pallas kernels for 0% -> 0%
where the time goes in v1:
time: 261 us; the launch traced here: 260 us
  waiting for transfers between devices  139 us (53%)
  starting transfers between devices  44.8 us (17%)
  other arithmetic  28.1 us (11%)
  local copies, waits for them, and re-layouts  19.9 us (8%)
  matrix products  14.3 us (5%)
  between operations  14.3 us (5%)
    all_to_all x1, waiting for transfers between devices, summed_on_arrival(): blocks = lax.all_to_all(split_up(shard, dim, peers), axis, 0, 0, tiled=True)  54.4 us
    all_to_all x1, waiting for transfers between devices, expert_half(): lax.all_to_all(outgoing, EP, split_axis=1, concat_axis=1, tiled=True)  47.7 us
    ppermute x1, waiting for transfers between devices, extended(): lax.ppermute(lax.slice_in_dim(block, block.shape[dim] - width, None, axis...  22.3 us
    all_to_all x1, starting transfers between devices, expert_half(): lax.all_to_all(outgoing, EP, split_axis=1, concat_axis=1, tiled=True)  13.7 us
    all_to_all x2, waiting for transfers between devices, moved_by_axis(): out = lax.all_to_all(out, axes[k], k, k, tiled=True)  10.4 us
    all_to_all x1, starting transfers between devices, summed_on_arrival(): blocks = lax.all_to_all(split_up(shard, dim, peers), axis, 0, 0, tiled=True)  9.75 us
    all_to_all x1, starting transfers between devices, expert_half(): lax.all_to_all(jnp.stack([returned] * lax.axis_size('tp')), 'tp', 0, 0)  8.65 us
    le x14, other arithmetic, mixer_half(): offset >= -half_span  7.9 us
  transfers between devices with their start and end apart: 9, of which 6 were waited for; matrix products, arithmetic and copies ran while one was open for 16% of the time, Pallas kernels for 0%

profile of v1, /device:TPU:1, one launch (start us, length us, event | category | flops | bytes accessed | tf_op | source)
XLA Modules:
  0.0 260.3 jit_solution(1649798705841614774)
XLA Ops:
  7.2 0.9 copy.31
  8.5 0.6 reduce-window.6
  9.4 1.4 scatter_custom_fusion
  10.9 1.2 fusion.5
  12.3 1.2 fusion.7
  13.5 2.5 gather_fusion
  16.0 3.8 %copy_select_fusion = bf16[16,32,2048]{2,0,1:T(8,128)(2,1)} fusion(bf16[16,32,2048]{2,1,0:T(8,128)(2,1)S(1)} %bitcast.56, pred[16,32]{0,1:T(8,128)(4,1)S(1)} %copy.35), kind=kLoop, calls=%fused_computation.5 | loop fusion | flops 1048576 | bytes 4194816 | tf_op jit(solution)/shard_map/jit(_where)/select_n | solution.py:124
  19.8 13.7 %all-to-all-start = ((bf16[16,32,2048]{2,0,1:T(8,128)(2,1)}), bf16[16,32,2048]{2,0,1:T(8,128)(2,1)S(1)}, u32[]{:S(2)}, u32[]{:S(2)}) async-start(bf16[16,32,2048]{2,0,1:T(8,128)(2,1)} %copy_select_fusion), calls=%async_computation | async-start | bytes 4194304 | tf_op jit(solution)/shard_map/all_to_all | solution.py:130
  33.6 0.7 all-gather.3.cloned.1.call-update
  34.3 47.7 %all-to-all-done = bf16[16,32,2048]{2,0,1:T(8,128)(2,1)S(1)} async-done(((bf16[16,32,2048]{2,0,1:T(8,128)(2,1)}), bf16[16,32,2048]{2,0,1:T(8,128)(2,1)S(1)}, u32[]{:S(2)}, u32[]{:S(2)}) %all-to-all-start) | async-done | bytes 2097184 | tf_op jit(solution)/shard_map/all_to_all | solution.py:130
  82.0 1.2 copy.37
  83.2 1.4 copy-done.1
  84.5 0.8 fusion.13
  85.7 4.5 %convolution_convert_fusion = bf16[512,2048]{1,0:T(8,128)(2,1)} fusion(bf16[512,2048]{1,0:T(8,128)(2,1)} %bitcast.59, bf16[1,224,2048]{2,1,0:T(8,128)(2,1)S(1)} %copy-done, bf16[1,2048,224]{1,2,0:T(8,128)(2,1)S(1)} %copy-done.8, f32[512,224]{0,1:T(8,128)S(1)} %fusion.13), kind=kOutput, calls=%fused_computation.3 | convolution fusion | flops 941260800 | bytes 6488064 | tf_op jit(solution)/shard_map/dot_general | solution.py:139
  90.2 9.8 %all-to-all-start.1 = ((bf16[16,32,2048]{2,1,0:T(8,128)(2,1)}), bf16[16,32,2048]{2,1,0:T(8,128)(2,1)S(1)}, u32[]{:S(2)}, u32[]{:S(2)}) async-start(bf16[16,32,2048]{2,1,0:T(8,128)(2,1)} %bitcast.57), calls=%async_computation.1 | async-start | bytes 4194304 | tf_op jit(solution)/shard_map/all_to_all | solution.py:35
  100.0 0.7 all-gather.5.cloned.1.call-update
  100.7 0.6 fusion.156
  101.3 0.6 fusion.158
  102.5 0.6 fusion.162
  103.1 54.4 %all-to-all-done.1 = bf16[16,32,2048]{2,1,0:T(8,128)(2,1)S(1)} async-done(((bf16[16,32,2048]{2,1,0:T(8,128)(2,1)}), bf16[16,32,2048]{2,1,0:T(8,128)(2,1)S(1)}, u32[]{:S(2)}, u32[]{:S(2)}) %all-to-all-start.1) | async-done | bytes 2097184 | tf_op jit(solution)/shard_map/all_to_all | solution.py:35
  158.0 0.7 reshape_transpose_reshape_reshape.3
  158.7 3.7 %all-to-all-start.2 = ((bf16[8,4,1,1,2048]{4,1,3,2,0:T(4,128)(2,1)}), bf16[8,4,1,1,2048]{4,1,3,2,0:T(4,128)(2,1)S(1)}, u32[]{:S(2)}, u32[]{:S(2)}) async-start(bf16[8,4,1,1,2048]{4,1,3,2,0:T(4,128)(2,1)} %reshape_transpose_reshape_reshape.3), calls=%async_computation.2 | async-start | bytes 262144 | tf_op jit(solution)/shard_map/all_to_all | solution.py:49
  163.0 0.6 fusion.166
  163.5 0.6 fusion.154
  164.2 6.1 %all-to-all-done.2 = bf16[8,4,1,1,2048]{4,1,3,2,0:T(4,128)(2,1)S(1)} async-done(((bf16[8,4,1,1,2048]{4,1,3,2,0:T(4,128)(2,1)}), bf16[8,4,1,1,2048]{4,1,3,2,0:T(4,128)(2,1)S(1)}, u32[]{:S(2)}, u32[]{:S(2)}) %all-to-all-start.2) | async-done | bytes 131104 | tf_op jit(solution)/shard_map/all_to_all | solution.py:49
  170.3 0.7 copy.38
  171.0 3.5 %all-to-all-start.3 = ((bf16[8,4,1,1,2048]{4,0,3,2,1:T(8,128)(2,1)}), bf16[8,4,1,1,2048]{4,0,3,2,1:T(8,128)(2,1)S(1)}, u32[]{:S(2)}, u32[]{:S(2)}) async-start(bf16[8,4,1,1,2048]{4,0,3,2,1:T(8,128)(2,1)} %copy.38), calls=%async_computation.3 | async-start | bytes 262144 | tf_op jit(solution)/shard_map/all_to_all | solution.py:49
  175.1 4.2 %all-to-all-done.3 = bf16[8,4,1,1,2048]{4,0,3,2,1:T(8,128)(2,1)S(1)} async-done(((bf16[8,4,1,1,2048]{4,0,3,2,1:T(8,128)(2,1)}), bf16[8,4,1,1,2048]{4,0,3,2,1:T(8,128)(2,1)S(1)}, u32[]{:S(2)}, u32[]{:S(2)}) %all-to-all-start.3) | async-done | bytes 131104 | tf_op jit(solution)/shard_map/all_to_all | solution.py:49
  179.5 1.6 stack.3
  181.1 8.6 %all-to-all-start.4 = ((bf16[16,1,32,2048]{3,2,1,0:T(8,128)(2,1)}), bf16[16,1,32,2048]{3,2,1,0:T(8,128)(2,1)S(1)}, u32[]{:S(2)}, u32[]{:S(2)}) async-start(bf16[16,1,32,2048]{3,2,1,0:T(8,128)(2,1)} %stack.3), calls=%async_computation.4 | async-start | bytes 4194304 | tf_op jit(solution)/shard_map/all_to_all | solution.py:146
  193.1 0.6 broadcast_compare_fusion.13
  193.7 0.6 broadcast_compare_fusion.15
  197.1 0.6 broadcast_compare_fusion.27
  198.2 0.6 pad_clamp_fusion
  199.6 2.0 multiply_bitcast_fusion
  201.6 2.4 convolution_convert_fusion.2
  204.1 0.6 fusion.174
  204.7 3.5 %collective-permute-start = (bf16[8,512]{1,0:T(8,128)(2,1)}, bf16[8,512]{1,0:T(8,128)(2,1)S(1)}, u32[]{:S(2)}, u32[]{:S(2)}) collective-permute-start(bf16[8,512]{1,0:T(8,128)(2,1)} %get-tuple-element.6), channel_id=1, source_target_pairs={{0,1},{1,2},{2,3},{3,4},{4,5},{5,6},{6,7},{7,8},{8,9},{9,10},{10,1... | collective-permute-start | bytes 24584 | tf_op jit(solution)/shard_map/ppermute | solution.py:19
  208.3 1.9 collective-permute-start.1
  210.7 1.9 reshape.527
  212.6 22.3 %collective-permute-done = bf16[8,512]{1,0:T(8,128)(2,1)S(1)} collective-permute-done((bf16[8,512]{1,0:T(8,128)(2,1)}, bf16[8,512]{1,0:T(8,128)(2,1)S(1)}, u32[]{:S(2)}, u32[]{:S(2)}) %collective-permute-start) | collective-permute-done | bytes 8224 | tf_op jit(solution)/shard_map/ppermute | solution.py:19
  234.9 2.8 %collective-permute-done.1 = bf16[8,512]{1,0:T(8,128)(2,1)S(1)} collective-permute-done((bf16[8,512]{1,0:T(8,128)(2,1)}, bf16[8,512]{1,0:T(8,128)(2,1)S(1)}, u32[]{:S(2)}, u32[]{:S(2)}) %collective-permute-start.1) | collective-permute-done | bytes 8224 | tf_op jit(solution)/shard_map/ppermute | solution.py:22
  237.7 1.6 maximum_convert_fusion
  239.3 6.6 %convolution_convert_fusion.1 = bf16[128,2048]{1,0:T(8,128)(2,1)} fusion(bf16[512,2048]{1,0:T(8,128)(2,1)} %all-gather.5.cloned.1.call-done, bf16[512,512]{1,0:T(8,128)(2,1)S(1)} %reshape.527, f32[144,512]{1,0:T(8,128)} %maximum_convert_fusion, f32[512]{0:T(512)} %param.17, f32[512]{0:T(512)} %get-tuple-element.53, pred[512]{0:T(512)(128)(4,1)} %get-tuple-element.23, ...), kind=kOutput, calls=%fused_computation.4 | convolution fusion | flops 342097920 | bytes 7367680 | tf_op jit(solution)/shard_map/dot_general | solution.py:100
  245.9 2.5 gather_fusion.1
  248.4 1.7 reshape.532
  250.2 1.5 fusion.173
  251.7 1.8 fusion.9
  (62 shorter events, 11.7 us)
Async XLA Ops:
  7.2 78.2 %copy-start = (bf16[1,224,2048]{2,1,0:T(8,128)(2,1)S(1)}, bf16[1,224,2048]{2,1,0:T(8,128)(2,1)}, u32[]{:S(2)}) copy-start(bf16[1,224,2048]{2,1,0:T(8,128)(2,1)} %param.25) | copy-start | bytes 2752516
  19.8 62.2 %all-to-all-start = ((bf16[16,32,2048]{2,0,1:T(8,128)(2,1)}), bf16[16,32,2048]{2,0,1:T(8,128)(2,1)S(1)}, u32[]{:S(2)}, u32[]{:S(2)}) async-start(bf16[16,32,2048]{2,0,1:T(8,128)(2,1)} %copy_select_fusion), calls=%async_computation | async-start | bytes 4194304 | tf_op jit(solution)/shard_map/all_to_all | solution.py:130
  33.5 168.1 %all-gather.3.cloned.1.call-start = ((), (), s32[]{:S(2)}) async-start(), calls=%async_computation.5 | async-start | bytes 2228224 | tf_op jit(solution)/shard_map/all_gather | solution.py:69
  82.0 2.5 copy-start.7
  83.2 1.4 copy-start.1
  84.5 1.2 copy-start.8
  90.2 67.3 %all-to-all-start.1 = ((bf16[16,32,2048]{2,1,0:T(8,128)(2,1)}), bf16[16,32,2048]{2,1,0:T(8,128)(2,1)S(1)}, u32[]{:S(2)}, u32[]{:S(2)}) async-start(bf16[16,32,2048]{2,1,0:T(8,128)(2,1)} %bitcast.57), calls=%async_computation.1 | async-start | bytes 4194304 | tf_op jit(solution)/shard_map/all_to_all | solution.py:35
  100.0 139.3 %all-gather.5.cloned.1.call-start = ((), (), s32[]{:S(2)}) async-start(), calls=%async_computation.6 | async-start | bytes 2228224 | tf_op jit(solution)/shard_map/all_gather | solution.py:102
  158.7 11.6 %all-to-all-start.2 = ((bf16[8,4,1,1,2048]{4,1,3,2,0:T(4,128)(2,1)}), bf16[8,4,1,1,2048]{4,1,3,2,0:T(4,128)(2,1)S(1)}, u32[]{:S(2)}, u32[]{:S(2)}) async-start(bf16[8,4,1,1,2048]{4,1,3,2,0:T(4,128)(2,1)} %reshape_transpose_reshape_reshape.3), calls=%async_computation.2 | async-start | bytes 262144 | tf_op jit(solution)/shard_map/all_to_all | solution.py:49
  171.0 8.3 %all-to-all-start.3 = ((bf16[8,4,1,1,2048]{4,0,3,2,1:T(8,128)(2,1)}), bf16[8,4,1,1,2048]{4,0,3,2,1:T(8,128)(2,1)S(1)}, u32[]{:S(2)}, u32[]{:S(2)}) async-start(bf16[8,4,1,1,2048]{4,0,3,2,1:T(8,128)(2,1)} %copy.38), calls=%async_computation.3 | async-start | bytes 262144 | tf_op jit(solution)/shard_map/all_to_all | solution.py:49
  181.1 17.7 %copy-start.2 = (bf16[128,2048]{1,0:T(8,128)(2,1)S(1)}, bf16[128,2048]{1,0:T(8,128)(2,1)}, u32[]{:S(2)}) copy-start(bf16[128,2048]{1,0:T(8,128)(2,1)} %param.13) | copy-start | bytes 1572868
  181.1 17.9 %copy-start.6 = (f32[128,2]{0,1:T(2,128)S(1)}, f32[128,2]{0,1:T(2,128)}, u32[]{:S(2)}) copy-start(f32[128,2]{0,1:T(2,128)} %param.22) | copy-start | bytes 3076
  181.1 64.8 %all-to-all-start.4 = ((bf16[16,1,32,2048]{3,2,1,0:T(8,128)(2,1)}), bf16[16,1,32,2048]{3,2,1,0:T(8,128)(2,1)S(1)}, u32[]{:S(2)}, u32[]{:S(2)}) async-start(bf16[16,1,32,2048]{3,2,1,0:T(8,128)(2,1)} %stack.3), calls=%async_computation.4 | async-start | bytes 4194304 | tf_op jit(solution)/shard_map/all_to_all | solution.py:146
  204.1 6.1 %copy-start.3 = (bf16[128,512]{1,0:T(8,128)(2,1)}, bf16[128,512]{1,0:T(8,128)(2,1)S(1)}, u32[]{:S(2)}) copy-start(bf16[128,512]{1,0:T(8,128)(2,1)S(1)} %convolution_convert_fusion.2) | copy-start | bytes 393220
  204.7 30.2 %collective-permute-start = (bf16[8,512]{1,0:T(8,128)(2,1)}, bf16[8,512]{1,0:T(8,128)(2,1)S(1)}, u32[]{:S(2)}, u32[]{:S(2)}) collective-permute-start(bf16[8,512]{1,0:T(8,128)(2,1)} %get-tuple-element.6), channel_id=1, source_target_pairs={{0,1},{1,2},{2,3},{3,4},{4,5},{5,6},{6,7},{7,8},{8,9},{9,10},{10,1... | collective-permute-start | bytes 24584 | tf_op jit(solution)/shard_map/ppermute | solution.py:19
  208.3 29.4 %collective-permute-start.1 = (bf16[8,512]{1,0:T(8,128)(2,1)}, bf16[8,512]{1,0:T(8,128)(2,1)S(1)}, u32[]{:S(2)}, u32[]{:S(2)}) collective-permute-start(bf16[8,512]{1,0:T(8,128)(2,1)} %get-tuple-element.7), channel_id=1, source_target_pairs={{1,0},{2,1},{3,2},{4,3},{5,4},{6,5},{7,6},{8,7},{9,8},{10,9},{11,1... | collective-permute-start | bytes 24584 | tf_op jit(solution)/shard_map/ppermute | solution.py:22
  250.2 1.5 copy-start.4
  250.2 1.5 copy-start.5
Sparse Core Ops, SparseCore 0:
  36.5 43.6 all-gather.2
  102.9 57.5 all-gather.4
